TPU v7x, 256 devices: a whole 4x4x8 slice. The times are simulated.
256 devices in a mesh: sp: 16 (over y, x), tp: 16 (over z, core).
Axes of the slice: x: 4, y: 4, z: 8, core: 2. Of those that a mesh axis runs over, the one named last changes fastest.
Arguments:
- latent: bfloat16 [8192, 4096], P(('sp', 'tp')), may hold values from -6 to 6
- context: bfloat16 [512, 4096], P('sp'), may hold values from -6 to 6
- condition: float32 [4096], replicated, may hold values from -6 to 6
- context_condition: float32 [4096], replicated, may hold values from -6 to 6
- modulation: bfloat16 [3, 4096, 4096], P(None, 'sp', 'tp'), may hold values from -0.09375 to 0.09375
- query_weight: bfloat16 [4096, 4096], P(None, 'tp'), as said below
- key_weight: bfloat16 [4096, 4096], P(None, 'tp'), as said below
- value_weight: bfloat16 [4096, 4096], P(None, 'tp'), may hold values from -0.09375 to 0.09375
- lambdas: float32 [16], P('tp'), may hold values from 0.3 to 0.8
- context_lift: float32 [16], P('tp'), may hold values from 1.5 to 3
- head_gain: float32 [256], replicated, may hold values from 0.1 to 1.9
- output_weight: bfloat16 [4096, 4096], P('tp'), may hold values from -0.09375 to 0.09375
Outputs:
- result: bfloat16 [8192, 4096], P(('sp', 'tp'))
Inputs may be any that keep to these rules, and one draw needn't show every extreme that they name: `query_weight`: entries lie within 200 / sqrt(4096) in magnitude. `key_weight`: entries lie within 6 / sqrt(4096) in magnitude.
All inputs are finite; a program needn't handle non-finite values.
Results may differ from a plain program's by a relative error of at most 0.025.
Values may be sent and summed in bfloat16 or wider, within the bound.
A program may use at most 64 MiB of HBM per device.

v0:
```python
import functools
import math
import jax
import jax.numpy as jnp
from jax import lax
from jax.sharding import Mesh
from jax.sharding import PartitionSpec as P

GRID_W = 64
SP = ("sp_0", "sp_1")
SP_TP = ("sp_0", "sp_1", "tp")
ROPE_BASE = 10000.0
EPSILON = 1e-05


def by_axis(shard, axes):
    return functools.reduce(lax.psum, axes, shard)


def from_everyone(shard, axis):
    copies = jnp.broadcast_to(shard, (lax.axis_size(axis), *shard.shape))
    return lax.all_to_all(copies, axis, split_axis=0, concat_axis=0, tiled=True)


def laid_out(pieces, dim):
    pieces = jnp.moveaxis(pieces, 0, dim)
    lengths = pieces.shape
    return pieces.reshape(*lengths[:dim], lengths[dim] * lengths[dim + 1], *lengths[dim + 2 :])


def collect(shard, axis, dim):
    pieces = from_everyone(shard, axis)
    return laid_out(pieces, dim)


def modulate(tokens_in, offset, scaling):
    values = tokens_in.astype(jnp.float32)
    center = jnp.mean(values, axis=-1, keepdims=True)
    spread = jnp.mean(jnp.square(values - center), axis=-1, keepdims=True)
    normed = (values - center) * lax.rsqrt(spread + EPSILON)
    return (normed * (1.0 + scaling) + offset).astype(jnp.bfloat16)


def rotate(tensor, places):
    number, head_count, head_width = tensor.shape
    quarter = head_width // 4
    eighth = head_width // 8
    inverse = ROPE_BASE ** (-jnp.arange(eighth, dtype=jnp.float32) / eighth)
    grid_row = (places // GRID_W).astype(jnp.float32)
    grid_col = (places % GRID_W).astype(jnp.float32)
    angles = jnp.stack([grid_row[:, None] * inverse, grid_col[:, None] * inverse], axis=1)
    cosine = jnp.cos(angles)[:, None, None, :, :]
    sine_table = jnp.sin(angles)[:, None, None, :, :]
    pieces = tensor.reshape(number, head_count, 2, 2, quarter)
    first_half = pieces[..., :eighth]
    second = pieces[..., eighth:]
    turned = jnp.concatenate(
        [first_half * cosine - second * sine_table, second * cosine + first_half * sine_table],
        axis=-1,
    )
    return turned.reshape(number, head_count, head_width)


def absorb(state_in, key_block, queries, lift_term, scale_factor):
    running_max, running_sum, running_out = state_in
    key_count = key_block.shape[0]
    head_count = queries.shape[1]
    head_width = 2 * queries.shape[3]
    local_width = head_count * head_width
    key_part = key_block[:, :local_width].reshape(key_count, head_count, 2, head_width // 2)
    value_part = key_block[:, local_width:].reshape(key_count, head_count, head_width)
    scores = (
        jnp.einsum("qhmd,khmd->mqhk", queries, key_part, preferred_element_type=jnp.float32)
        * scale_factor
        + lift_term
    )
    new_max = jnp.maximum(running_max, jnp.max(scores, axis=-1))
    fading = jnp.exp(running_max - new_max)
    weights = jnp.exp(scores - new_max[..., None])
    new_sum = running_sum * fading + jnp.sum(weights, axis=-1)
    new_out = running_out * fading[..., None] + jnp.einsum(
        "mqhk,khd->mqhd",
        weights.astype(jnp.bfloat16),
        value_part,
        preferred_element_type=jnp.float32,
    )
    return (new_max, new_sum, new_out)


def shards(
    latent,
    context,
    condition,
    context_condition,
    modulation,
    query_weight,
    key_weight,
    value_weight,
    lambdas,
    context_lift,
    head_gain,
    output_weight,
):
    sp_index = lax.axis_index(SP)
    rows_block = modulation.shape[1]
    silu_pair = jax.nn.silu(jnp.stack([condition, context_condition])).astype(jnp.bfloat16)
    own_rows = lax.dynamic_slice_in_dim(silu_pair, sp_index * rows_block, rows_block, 1)
    partial_mod = jnp.einsum(
        "cd,rde->cre", own_rows, modulation, preferred_element_type=jnp.float32
    )
    summed = by_axis(partial_mod, SP)
    mod_vectors = collect(summed, "tp", 2)
    head_count = lambdas.shape[0]
    head_width = query_weight.shape[1] // head_count
    half_width = head_width // 2
    local_width = head_count * head_width
    scale_factor = half_width ** (-0.5)
    normed = modulate(latent, mod_vectors[0, 0], mod_vectors[0, 1])
    projection = jnp.concatenate([query_weight, key_weight, value_weight], axis=1)
    projected = jnp.dot(
        lax.all_gather(normed, "tp", axis=0, tiled=True),
        projection,
        preferred_element_type=jnp.float32,
    ).astype(jnp.bfloat16)
    block_tokens = projected.shape[0]
    places = sp_index * block_tokens + jnp.arange(block_tokens, dtype=jnp.int32)
    queries = rotate(
        projected[:, :local_width]
        .astype(jnp.float32)
        .reshape(block_tokens, head_count, head_width),
        places,
    )
    queries = queries.astype(jnp.bfloat16).reshape(block_tokens, head_count, 2, half_width)
    latent_keys = rotate(
        projected[:, local_width : 2 * local_width]
        .astype(jnp.float32)
        .reshape(block_tokens, head_count, head_width),
        places,
    )
    latent_keys = latent_keys.astype(jnp.bfloat16).reshape(block_tokens, local_width)
    packed = jnp.concatenate([latent_keys, projected[:, 2 * local_width :]], axis=1)
    normed_context = modulate(context, mod_vectors[1, 0], mod_vectors[1, 1])
    own_context = jnp.dot(
        normed_context, projection[:, local_width:], preferred_element_type=jnp.float32
    ).astype(jnp.bfloat16)
    context_packed = collect(own_context, SP, 0)
    initial = (
        jnp.full((2, block_tokens, head_count), -jnp.inf, jnp.float32),
        jnp.zeros((2, block_tokens, head_count), jnp.float32),
        jnp.zeros((2, block_tokens, head_count, head_width), jnp.float32),
    )
    state_now = absorb(initial, context_packed, queries, context_lift[:, None], scale_factor)
    segment = lax.all_gather(packed, SP, axis=0, tiled=True)
    length = segment.shape[0]
    block_len = math.gcd(length, 1024)
    stacked = segment.reshape(length // block_len, block_len, segment.shape[1])

    def one_block(state_step, block_rows):
        return (absorb(state_step, block_rows, queries, 0.0, scale_factor), None)

    running_max, running_sum, running_out = lax.scan(one_block, state_now, stacked)[0]
    means = running_out / running_sum[..., None]
    difference = means[0] - lambdas[None, :, None] * means[1]
    scaled = (
        difference
        * lax.rsqrt(jnp.mean(jnp.square(difference), axis=-1, keepdims=True) + EPSILON)
        * head_gain
    )
    attended = scaled.astype(jnp.bfloat16).reshape(block_tokens, local_width)
    mixture = lax.psum_scatter(
        jnp.dot(attended, output_weight, preferred_element_type=jnp.float32).astype(jnp.bfloat16),
        "tp",
        scatter_dimension=0,
        tiled=True,
    ).astype(jnp.float32)
    return (latent.astype(jnp.float32) + mod_vectors[0, 2] * mixture).astype(jnp.bfloat16)


def solution(mesh):
    split = Mesh(mesh.devices.reshape(4, 4, mesh.shape["tp"]), ("sp_0", "sp_1", "tp"))
    return jax.shard_map(
        shards,
        mesh=split,
        in_specs=(
            P(SP_TP, None),
            P(SP, None),
            P(),
            P(),
            P(None, SP, "tp"),
            P(None, "tp"),
            P(None, "tp"),
            P(None, "tp"),
            P("tp"),
            P("tp"),
            P(),
            P("tp", None),
        ),
        out_specs=P(SP_TP, None),
        check_vma=False,
    )
```

profile of v0, /device:TPU:14, one launch (start us, length us, event | category | flops | bytes accessed | tf_op | source)
XLA Modules:
  0.0 305.2 jit_solution(5398257934742290326)
XLA Ops:
  6.5 1.4 fusion.78
  7.9 8.8 %psum.14 = f32[2,3,256]{2,0,1:T(2,128)S(1)} all-reduce(f32[2,3,256]{2,0,1:T(2,128)S(1)} %fusion.78), channel_id=1, replica_groups=mesh['sp_0'=4,'sp_1'=4,'tp'=16] {'sp_0'}, use_global_device_ids=true, to_apply=%region_0.1 | all-reduce | flops 1536 | bytes 12288 | tf_op jit(solution)/shard_map/psum | solution.py:17
  16.7 8.3 %psum.15 = f32[2,3,256]{2,0,1:T(2,128)S(1)} all-reduce(f32[2,3,256]{2,0,1:T(2,128)S(1)} %psum.14), channel_id=1, replica_groups=mesh['sp_0'=4,'sp_1'=4,'tp'=16] {'sp_1'}, use_global_device_ids=true, to_apply=%region_1.2 | all-reduce | flops 1536 | bytes 12288 | tf_op jit(solution)/shard_map/psum | solution.py:17
  25.7 7.9 %all-to-all-start = ((f32[16,2,3,256]{3,1,2,0:T(2,128)}), f32[16,2,3,256]{3,1,2,0:T(2,128)S(1)}, u32[]{:S(2)}, u32[]{:S(2)}) async-start(f32[16,2,3,256]{3,1,2,0:T(2,128)} %broadcast_in_dim.12), calls=%async_computation | async-start | bytes 196608 | tf_op jit(solution)/shard_map/all_to_all | solution.py:22
  35.9 6.0 %all-to-all-done = f32[16,2,3,256]{3,1,2,0:T(2,128)S(1)} async-done(((f32[16,2,3,256]{3,1,2,0:T(2,128)}), f32[16,2,3,256]{3,1,2,0:T(2,128)S(1)}, u32[]{:S(2)}, u32[]{:S(2)}) %all-to-all-start) | async-done | bytes 98336 | tf_op jit(solution)/shard_map/all_to_all | solution.py:22
  42.0 1.8 fusion.51
  44.4 38.9 %all-gather.3.cloned.1.call-done = bf16[512,4096]{1,0:T(8,128)(2,1)} async-done(((bf16[32,4096]{1,0:T(8,128)(2,1)}), bf16[512,4096]{1,0:T(8,128)(2,1)}) %all-gather.3.cloned.1.call-update) | async-done | bytes 4194320 | tf_op jit(solution)/shard_map/all_gather | solution.py:121
  83.4 7.5 %fusion.31 = bf16[512,768]{1,0:T(8,128)(2,1)S(1)} fusion(bf16[512,4096]{1,0:T(8,128)(2,1)} %all-gather.3.cloned.1.call-done, bf16[4096,256]{1,0:T(8,128)(2,1)} %param.21, bf16[4096,256]{1,0:T(8,128)(2,1)} %param.20, bf16[4096,256]{1,0:T(8,128)(2,1)} %param.19), kind=kOutput, calls=%fused_computation.37 | convolution fusion | flops 3240493056 | bytes 11272192 | tf_op jit(solution)/shard_map/dot_general | solution.py:120
  93.3 1.8 pad_maximum_fusion
  97.5 3.2 %fusion.36 = bf16[32,512]{1,0:T(8,128)(2,1)S(1)} fusion(bf16[4096,256]{1,0:T(8,128)(2,1)} %param.21, bf16[4096,256]{1,0:T(8,128)(2,1)} %param.20, bf16[32,4096]{1,0:T(8,128)(2,1)} %param.15, f32[4096]{0:T(1024)S(1)} %bitcast.171, f32[4096]{0:T(1024)S(1)} %bitcast.172, f32[32]{0:T(128)S(1)} %add_rsqrt_fusion.2, f32[32]{0:T(128)S(1)} %broadcast_multiply_fusion.3), kind=kOutput, calls=%fused_computation.41 | convolution fusion | flops 143409152 | bytes 4522240 | tf_op jit(solution)/shard_map/dot_general | solution.py:143
  101.6 7.2 %all-to-all-start.1 = ((bf16[16,32,512]{2,1,0:T(8,128)(2,1)}), bf16[16,32,512]{2,1,0:T(8,128)(2,1)S(1)}, u32[]{:S(2)}, u32[]{:S(2)}) async-start(bf16[16,32,512]{2,1,0:T(8,128)(2,1)} %broadcast_in_dim.13), calls=%async_computation.1 | async-start | bytes 1048576 | tf_op jit(solution)/shard_map/all_to_all | solution.py:22
  110.3 11.8 %all-to-all-done.1 = bf16[16,32,512]{2,1,0:T(8,128)(2,1)S(1)} async-done(((bf16[16,32,512]{2,1,0:T(8,128)(2,1)}), bf16[16,32,512]{2,1,0:T(8,128)(2,1)S(1)}, u32[]{:S(2)}, u32[]{:S(2)}) %all-to-all-start.1) | async-done | bytes 524320 | tf_op jit(solution)/shard_map/all_to_all | solution.py:22
  122.9 1.8 copy.35
  125.2 1.5 bitcast_reduce_fusion.1
  127.1 1.7 fusion.35
  128.9 43.7 %all-gather.5.cloned.1.call-done = bf16[8192,512]{1,0:T(8,128)(2,1)} async-done(((bf16[512,512]{1,0:T(8,128)(2,1)}), bf16[8192,512]{1,0:T(8,128)(2,1)}) %all-gather.5.cloned.1.call-update) | async-done | bytes 8388624 | tf_op jit(solution)/shard_map/all_gather | solution.py:153
  172.6 54.9 %while.14 = (s32[]{:T(128)}, f32[2,512,1]{1,0,2:T(2,128)S(1)}, f32[2,512,1]{1,0,2:T(2,128)S(1)}, f32[2,512,1,256]{1,3,0,2:T(8,128)}, bf16[8,1024,512]{2,1,0:T(8,...) while((s32[]{:T(128)}, f32[2,512,1]{1,0,2:T(2,128)S(1)}, f32[2,512,1]{1,0,2:T(2,128)S(1)}, ...), condition=%wide.region_11.12_spmd, body=%wide.region_8.11_spmd.sunk | while | flops 814222336 | bytes 33882276 | solution.py:161
  173.9 1.3 copy.54
  180.7 1.3 copy.54
  187.6 1.3 copy.54
  227.5 1.4 broadcast_divide_fusion
  229.0 3.3 %convolution_convert_fusion = bf16[512,4096]{1,0:T(8,128)(2,1)} fusion(bf16[256,4096]{1,0:T(8,128)(2,1)S(1)} %copy-done, f32[256]{0:T(256)S(1)} %copy-done.7, f32[512]{0:T(512)S(1)} %add_rsqrt_fusion, f32[2,512,1,256]{1,3,0,2:T(8,128)S(1)} %broadcast_divide_fusion, f32[]{:T(128)} %bitcast.145), kind=kOutput, calls=%fused_computation.26 | convolution fusion | flops 1076494336 | bytes 7343108 | tf_op jit(solution)/shard_map/dot_general | solution.py:171
  232.3 64.6 %reduce-scatter.2.cloned.1.call-done = bf16[32,4096]{1,0:T(8,128)(2,1)} async-done(((bf16[512,4096]{1,0:T(8,128)(2,1)}), bf16[32,4096]{1,0:T(8,128)(2,1)}) %reduce-scatter.2.cloned.1.call-update) | async-done | bytes 262160 | tf_op jit(solution)/shard_map/reduce_scatter | solution.py:170
  296.9 1.7 fusion.56
  (164 shorter events, 62.0 us)
Async XLA Ops:
  6.5 222.5 %copy-start = (bf16[256,4096]{1,0:T(8,128)(2,1)S(1)}, bf16[256,4096]{1,0:T(8,128)(2,1)}, u32[]{:S(2)}) copy-start(bf16[256,4096]{1,0:T(8,128)(2,1)} %param.25) | copy-start | bytes 6291460
  25.7 16.2 %all-to-all-start = ((f32[16,2,3,256]{3,1,2,0:T(2,128)}), f32[16,2,3,256]{3,1,2,0:T(2,128)S(1)}, u32[]{:S(2)}, u32[]{:S(2)}) async-start(f32[16,2,3,256]{3,1,2,0:T(2,128)} %broadcast_in_dim.12), calls=%async_computation | async-start | bytes 196608 | tf_op jit(solution)/shard_map/all_to_all | solution.py:22
  33.6 49.8 %all-gather.3.cloned.1.call-start = ((), (), s32[]{:S(2)}) async-start(), calls=%async_computation.3 | async-start | bytes 4456448 | tf_op jit(solution)/shard_map/all_gather | solution.py:121
  43.8 128.8 %all-gather.5.cloned.1.call-start = ((), (), s32[]{:S(2)}) async-start(), calls=%async_computation.4 | async-start | bytes 8912896 | tf_op jit(solution)/shard_map/all_gather | solution.py:153
  101.6 20.5 %all-to-all-start.1 = ((bf16[16,32,512]{2,1,0:T(8,128)(2,1)}), bf16[16,32,512]{2,1,0:T(8,128)(2,1)S(1)}, u32[]{:S(2)}, u32[]{:S(2)}) async-start(bf16[16,32,512]{2,1,0:T(8,128)(2,1)} %broadcast_in_dim.13), calls=%async_computation.1 | async-start | bytes 1048576 | tf_op jit(solution)/shard_map/all_to_all | solution.py:22
  108.8 188.1 %reduce-scatter.2.cloned.1.call-start = ((), (), s32[]{:S(2)}) async-start(), calls=%async_computation.5 | async-start | bytes 4456448 | tf_op jit(solution)/shard_map/reduce_scatter | solution.py:170
  122.1 2.6 copy-start.5
  125.0 2.1 copy-start.6
  172.6 56.4 %copy-start.7 = (f32[256]{0:T(256)S(1)}, f32[256]{0:T(256)}, u32[]{:S(2)}) copy-start(f32[256]{0:T(256)} %param.24) | copy-start | bytes 3076
  175.2 2.0 copy-start.1
  175.2 2.0 copy-start.2
  182.1 2.0 copy-start.1
  182.1 2.0 copy-start.2
  188.9 2.0 copy-start.1
  188.9 2.0 copy-start.2
  195.8 2.0 copy-start.2
  202.6 2.0 copy-start.2
  209.5 2.0 copy-start.1
  209.5 2.0 copy-start.2
  216.4 2.0 copy-start.1
  216.4 2.0 copy-start.2
  223.2 2.0 copy-start.1
  223.2 2.0 copy-start.2
  229.0 67.9 %copy-start.4 = (bf16[32,4096]{1,0:T(8,128)(2,1)S(1)}, bf16[32,4096]{1,0:T(8,128)(2,1)}, u32[]{:S(2)}) copy-start(bf16[32,4096]{1,0:T(8,128)(2,1)} %param.14) | copy-start | bytes 786436
  (10 other events, 12.6 us)
Sparse Core Ops, SparseCore 0:
  43.9 39.4 all-gather.2
  95.3 77.2 all-gather.4
  232.5 64.4 reduce-scatter.1
where the time goes:
time: 306 us; the launch traced here: 305 us
  waiting for transfers between devices  165 us (54%)
  local copies, waits for them, and re-layouts  39.2 us (13%)
  matrix products  33.8 us (11%)
  other arithmetic  19.6 us (6%)
  blocking collectives  17.1 us (6%)
  starting transfers between devices  15.4 us (5%)
  between operations  14.6 us (5%)
    reduce_scatter x1, waiting for transfers between devices, shards(): lax.psum_scatter(jnp.dot(attended, output_weight, preferred_element_type=...  64.6 us
    all_gather x1, waiting for transfers between devices, shards(): segment = lax.all_gather(packed, SP, axis=0, tiled=True)  43.7 us
    all_gather x1, waiting for transfers between devices, shards(): lax.all_gather(normed, 'tp', axis=0, tiled=True)  38.9 us
    dynamic_slice x16, local copies, waits for them, and re-layouts, shards(): lax.scan(one_block, state_now, stacked)[0]  20.8 us
    all_to_all x2, waiting for transfers between devices, from_everyone(): return lax.all_to_all(copies, axis, split_axis=0, concat_axis=0, tiled=True)  17.7 us
    psum x2, blocking collectives, by_axis(): return functools.reduce(lax.psum, axes, shard)  17.1 us
    all_to_all x2, starting transfers between devices, from_everyone(): return lax.all_to_all(copies, axis, split_axis=0, concat_axis=0, tiled=True)  15.1 us
    slice x10, local copies, waits for them, and re-layouts, absorb(): key_block[:, :local_width]  12.4 us
  transfers between devices with their start and end apart: 5, of which 5 were waited for; matrix products, arithmetic and copies ran while one was open for 5% of the time, Pallas kernels for 0%

commit v1 on v0

--- a/solution.py
+++ b/solution.py
@@ -150,7 +150,9 @@
         jnp.zeros((2, block_tokens, head_count, head_width), jnp.float32),
     )
     state_now = absorb(initial, context_packed, queries, context_lift[:, None], scale_factor)
-    segment = lax.all_gather(packed, SP, axis=0, tiled=True)
+    segment = jnp.concatenate(
+        lax.all_to_all(jnp.stack([packed] * lax.axis_size(SP)), SP, 0, 0), axis=0
+    )
     length = segment.shape[0]
     block_len = math.gcd(length, 1024)
     stacked = segment.reshape(length // block_len, block_len, segment.shape[1])

time: 306 us -> 361 us (1.18)
  waiting for transfers between devices: 165 us -> 206 us
  starting transfers between devices: 15.4 us -> 25 us
  local copies, waits for them, and re-layouts: 39.2 us -> 43.2 us
    all_to_all x0 -> x1, waiting for transfers between devices: none -> 113 us  [shards(): lax.all_to_all(jnp.stack([packed] * lax.axis_size(SP)), SP, 0, 0)]
    all_gather x1 -> x0, waiting for transfers between devices: 43.7 us -> none  [shards(): segment = lax.all_gather(packed, SP, axis=0, tiled=True)]
    all_gather x1, waiting for transfers between devices: 38.9 us -> 23 us  [shards(): lax.all_gather(normed, 'tp', axis=0, tiled=True)]
    all_to_all x2, waiting for transfers between devices: 17.7 us -> 5.95 us  [from_everyone(): return lax.all_to_all(copies, axis, split_axis=0, concat_axis=0, tiled=True)]
    all_to_all x0 -> x1, starting transfers between devices: none -> 7.24 us  [shards(): lax.all_to_all(jnp.stack([packed] * lax.axis_size(SP)), SP, 0, 0)]
    another operation x0 -> x1, local copies, waits for them, and re-layouts: none -> 4.02 us  [shards(): jnp.stack([packed] * lax.axis_size(SP))]
  transfers between devices with their start and end apart: 5 -> 5, of which waited for: 5 -> 4; matrix products, arithmetic and copies ran while one was open for 5% -> 8% of each run, Pallas kernels for 0% -> 0%
where the time goes in v1:
time: 361 us; the launch traced here: 360 us
  waiting for transfers between devices  206 us (57%)
  local copies, waits for them, and re-layouts  43.2 us (12%)
  matrix products  34.7 us (10%)
  starting transfers between devices  25 us (7%)
  other arithmetic  18.9 us (5%)
  blocking collectives  17.1 us (5%)
  between operations  14.9 us (4%)
    all_to_all x1, waiting for transfers between devices, shards(): lax.all_to_all(jnp.stack([packed] * lax.axis_size(SP)), SP, 0, 0)  113 us
    reduce_scatter x1, waiting for transfers between devices, shards(): lax.psum_scatter(jnp.dot(attended, output_weight, preferred_element_type=...  63.9 us
    all_gather x1, waiting for transfers between devices, shards(): lax.all_gather(normed, 'tp', axis=0, tiled=True)  23 us
    dynamic_slice x16, local copies, waits for them, and re-layouts, shards(): lax.scan(one_block, state_now, stacked)[0]  21.5 us
    all_to_all x2, starting transfers between devices, from_everyone(): return lax.all_to_all(copies, axis, split_axis=0, concat_axis=0, tiled=True)  17.5 us
    psum x2, blocking collectives, by_axis(): return functools.reduce(lax.psum, axes, shard)  17.1 us
    dot_general x9, matrix products, absorb(): jnp.einsum('mqhk,khd->mqhd', weights.astype(jnp.bfloat16), value_part, pr...  11.7 us
    slice x10, local copies, waits for them, and re-layouts, absorb(): key_block[:, :local_width]  11.6 us
  transfers between devices with their start and end apart: 5, of which 4 were waited for; matrix products, arithmetic and copies ran while one was open for 8% of the time, Pallas kernels for 0%

profile of v1, /device:TPU:14, one launch (start us, length us, event | category | flops | bytes accessed | tf_op | source)
XLA Modules:
  0.0 360.0 jit_solution(11918117705345531628)
XLA Ops:
  6.5 1.4 fusion.78
  7.9 8.8 %psum.14 = f32[2,3,256]{2,0,1:T(2,128)S(1)} all-reduce(f32[2,3,256]{2,0,1:T(2,128)S(1)} %fusion.78), channel_id=1, replica_groups=mesh['sp_0'=4,'sp_1'=4,'tp'=16] {'sp_0'}, use_global_device_ids=true, to_apply=%region_0.1 | all-reduce | flops 1536 | bytes 12288 | tf_op jit(solution)/shard_map/psum | solution.py:17
  16.7 8.3 %psum.15 = f32[2,3,256]{2,0,1:T(2,128)S(1)} all-reduce(f32[2,3,256]{2,0,1:T(2,128)S(1)} %psum.14), channel_id=1, replica_groups=mesh['sp_0'=4,'sp_1'=4,'tp'=16] {'sp_1'}, use_global_device_ids=true, to_apply=%region_1.2 | all-reduce | flops 1536 | bytes 12288 | tf_op jit(solution)/shard_map/psum | solution.py:17
  25.7 7.9 %all-to-all-start = ((f32[16,2,3,256]{3,1,2,0:T(2,128)}), f32[16,2,3,256]{3,1,2,0:T(2,128)S(1)}, u32[]{:S(2)}, u32[]{:S(2)}) async-start(f32[16,2,3,256]{3,1,2,0:T(2,128)} %broadcast_in_dim.12), calls=%async_computation | async-start | bytes 196608 | tf_op jit(solution)/shard_map/all_to_all | solution.py:22
  35.9 6.0 %all-to-all-done = f32[16,2,3,256]{3,1,2,0:T(2,128)S(1)} async-done(((f32[16,2,3,256]{3,1,2,0:T(2,128)}), f32[16,2,3,256]{3,1,2,0:T(2,128)S(1)}, u32[]{:S(2)}, u32[]{:S(2)}) %all-to-all-start) | async-done | bytes 98336 | tf_op jit(solution)/shard_map/all_to_all | solution.py:22
  42.0 1.8 fusion.51
  46.7 3.2 fusion.36
  50.7 9.6 %all-to-all-start.1 = ((bf16[16,32,512]{2,1,0:T(8,128)(2,1)}), bf16[16,32,512]{2,1,0:T(8,128)(2,1)}, u32[]{:S(2)}, u32[]{:S(2)}) async-start(bf16[16,32,512]{2,1,0:T(8,128)(2,1)} %broadcast_in_dim.13), calls=%async_computation.1 | async-start | bytes 1048576 | tf_op jit(solution)/shard_map/all_to_all | solution.py:22
  60.4 23.0 %all-gather.2.cloned.1.call-done = bf16[512,4096]{1,0:T(8,128)(2,1)} async-done(((bf16[32,4096]{1,0:T(8,128)(2,1)}), bf16[512,4096]{1,0:T(8,128)(2,1)}) %all-gather.2.cloned.1.call-update) | async-done | bytes 4194320 | tf_op jit(solution)/shard_map/all_gather | solution.py:121
  83.4 7.5 %fusion.31 = bf16[512,768]{1,0:T(8,128)(2,1)S(1)} fusion(bf16[512,4096]{1,0:T(8,128)(2,1)} %all-gather.2.cloned.1.call-done, bf16[4096,256]{1,0:T(8,128)(2,1)} %param.21, bf16[4096,256]{1,0:T(8,128)(2,1)} %param.20, bf16[4096,256]{1,0:T(8,128)(2,1)} %param.19), kind=kOutput, calls=%fused_computation.37 | convolution fusion | flops 3240493056 | bytes 11272192 | tf_op jit(solution)/shard_map/dot_general | solution.py:120
  95.1 4.0 %stack.14 = bf16[16,512,512]{2,1,0:T(8,128)(2,1)} broadcast(bf16[512,512]{1,0:T(8,128)(2,1)S(1)} %pad_maximum_fusion), dimensions={1,2} | broadcast | bytes 8912896 | tf_op jit(solution)/shard_map/stack | solution.py:154
  99.1 7.2 %all-to-all-start.2 = ((bf16[16,512,512]{2,1,0:T(8,128)(2,1)}), bf16[16,512,512]{2,1,0:T(8,128)(2,1)}, u32[]{:S(2)}, u32[]{:S(2)}) async-start(bf16[16,512,512]{2,1,0:T(8,128)(2,1)} %stack.14), calls=%async_computation.2 | async-start | bytes 16777216 | tf_op jit(solution)/shard_map/all_to_all | solution.py:154
  110.2 1.5 bitcast_reduce_fusion.1
  112.1 2.6 fusion.35
  114.8 112.9 %all-to-all-done.2 = bf16[16,512,512]{2,1,0:T(8,128)(2,1)} async-done(((bf16[16,512,512]{2,1,0:T(8,128)(2,1)}), bf16[16,512,512]{2,1,0:T(8,128)(2,1)}, u32[]{:S(2)}, u32[]{:S(2)}) %all-to-all-start.2) | async-done | bytes 8388640 | tf_op jit(solution)/shard_map/all_to_all | solution.py:154
  227.6 55.0 %while.14 = (s32[]{:T(128)}, f32[2,512,1]{1,0,2:T(2,128)S(1)}, f32[2,512,1]{1,0,2:T(2,128)S(1)}, f32[2,512,1,256]{1,3,0,2:T(8,128)}, bf16[8,1024,512]{2,1,0:T(8,...) while((s32[]{:T(128)}, f32[2,512,1]{1,0,2:T(2,128)S(1)}, f32[2,512,1]{1,0,2:T(2,128)S(1)}, ...), condition=%wide.region_11.12_spmd, body=%wide.region_8.11_spmd.sunk | while | flops 814222336 | bytes 33882276 | solution.py:163
  228.9 1.4 copy.53
  235.8 1.4 copy.53
  242.7 1.4 copy.53
  249.5 1.4 copy.53
  277.0 1.4 copy.53
  284.1 3.3 convolution_convert_fusion
  287.5 63.9 %reduce-scatter.2.cloned.1.call-done = bf16[32,4096]{1,0:T(8,128)(2,1)} async-done(((bf16[512,4096]{1,0:T(8,128)(2,1)}), bf16[32,4096]{1,0:T(8,128)(2,1)}) %reduce-scatter.2.cloned.1.call-update) | async-done | bytes 262160 | tf_op jit(solution)/shard_map/reduce_scatter | solution.py:172
  351.4 1.7 fusion.56
  (160 shorter events, 63.1 us)
Async XLA Ops:
  6.5 277.6 %copy-start = (bf16[256,4096]{1,0:T(8,128)(2,1)S(1)}, bf16[256,4096]{1,0:T(8,128)(2,1)}, u32[]{:S(2)}) copy-start(bf16[256,4096]{1,0:T(8,128)(2,1)} %param.25) | copy-start | bytes 6291460
  25.7 16.2 %all-to-all-start = ((f32[16,2,3,256]{3,1,2,0:T(2,128)}), f32[16,2,3,256]{3,1,2,0:T(2,128)S(1)}, u32[]{:S(2)}, u32[]{:S(2)}) async-start(f32[16,2,3,256]{3,1,2,0:T(2,128)} %broadcast_in_dim.12), calls=%async_computation | async-start | bytes 196608 | tf_op jit(solution)/shard_map/all_to_all | solution.py:22
  33.6 49.8 %all-gather.2.cloned.1.call-start = ((), (), s32[]{:S(2)}) async-start(), calls=%async_computation.4 | async-start | bytes 4456448 | tf_op jit(solution)/shard_map/all_gather | solution.py:121
  50.7 44.4 %all-to-all-start.1 = ((bf16[16,32,512]{2,1,0:T(8,128)(2,1)}), bf16[16,32,512]{2,1,0:T(8,128)(2,1)}, u32[]{:S(2)}, u32[]{:S(2)}) async-start(bf16[16,32,512]{2,1,0:T(8,128)(2,1)} %broadcast_in_dim.13), calls=%async_computation.1 | async-start | bytes 1048576 | tf_op jit(solution)/shard_map/all_to_all | solution.py:22
  99.1 128.5 %all-to-all-start.2 = ((bf16[16,512,512]{2,1,0:T(8,128)(2,1)}), bf16[16,512,512]{2,1,0:T(8,128)(2,1)}, u32[]{:S(2)}, u32[]{:S(2)}) async-start(bf16[16,512,512]{2,1,0:T(8,128)(2,1)} %stack.14), calls=%async_computation.2 | async-start | bytes 16777216 | tf_op jit(solution)/shard_map/all_to_all | solution.py:154
  106.4 245.0 %reduce-scatter.2.cloned.1.call-start = ((), (), s32[]{:S(2)}) async-start(), calls=%async_computation.5 | async-start | bytes 4456448 | tf_op jit(solution)/shard_map/reduce_scatter | solution.py:172
  227.6 56.5 %copy-start.5 = (f32[256]{0:T(256)S(1)}, f32[256]{0:T(256)}, u32[]{:S(2)}) copy-start(f32[256]{0:T(256)} %param.24) | copy-start | bytes 3076
  230.3 2.0 copy-start.1
  230.3 2.0 copy-start.2
  237.2 2.0 copy-start.1
  237.2 2.0 copy-start.2
  244.1 2.0 copy-start.1
  244.1 2.0 copy-start.2
  250.9 2.0 copy-start.1
  250.9 2.0 copy-start.2
  257.8 2.0 copy-start.1
  257.8 2.0 copy-start.2
  264.7 2.0 copy-start.1
  264.7 2.0 copy-start.2
  271.6 2.0 copy-start.1
  271.6 2.0 copy-start.2
  278.4 2.0 copy-start.1
  278.4 2.0 copy-start.2
  284.1 67.3 %copy-start.4 = (bf16[32,4096]{1,0:T(8,128)(2,1)S(1)}, bf16[32,4096]{1,0:T(8,128)(2,1)}, u32[]{:S(2)}) copy-start(bf16[32,4096]{1,0:T(8,128)(2,1)} %param.14) | copy-start | bytes 786436
  (8 other events, 8.0 us)
Sparse Core Ops, SparseCore 0:
  43.9 39.4 all-gather.1
  287.6 63.7 reduce-scatter.1
